TPU v7x, 32 devices: a whole 2x2x4 slice. The times are simulated.
32 devices in a mesh: kv: 8 (over z, y), tp: 4 (over x, core).
Axes of the slice: x: 2, y: 2, z: 4, core: 2. Of those that a mesh axis runs over, the one named last changes fastest.
Arguments:
- queries: bfloat16 [2048, 3072], P('kv', 'tp'), may hold values from -6 to 6
- key_vectors: bfloat16 [2048, 512], P('kv', 'tp'), may hold values from -6 to 6
- value_vectors: bfloat16 [2048, 512], P('kv', 'tp'), may hold values from -6 to 6
- log_sums: float32 [2048, 48], P('kv', 'tp'), may hold values from 4.5 to 6.5
- out_grad: bfloat16 [2048, 3072], P('kv', 'tp'), may hold values from -48 to 48
- layer_input: bfloat16 [2048, 3072], P('kv', 'tp'), may hold values from -0.29882812 to 0.29882812
- chosen: int32 [32, 16], P('kv'), may hold values from -1 to 55, as said below
Outputs:
- query_grad: bfloat16 [2048, 3072], P('kv', 'tp')
- key_grad: bfloat16 [2048, 512], P('kv', 'tp')
- value_grad: bfloat16 [2048, 512], P('kv', 'tp')
- weight_grad: float32 [3072, 512], P('kv', 'tp')
Inputs may be any that keep to these rules, and one draw needn't show every extreme that they name: `chosen`: each entry is -1 or the number c of a block of 32 positions (c * 32 to c * 32 + 31) that lies wholly within an earlier index of kv than its query block. The numbers of one row differ, and all query blocks held by one index of kv together take at most one block from each other index.
All inputs are finite; a program needn't handle non-finite values.
Results may differ from a plain program's by a relative error of at most 0.0061.
Values may be sent and summed in bfloat16 or wider, within the bound.
No kernel may reach another device: no remote copies, remote signals or barrier semaphores. Data moves between devices by JAX's collectives and lax.ppermute only.
A program may use at most 64 MiB of HBM per device.

v0:
```python
import jax
import jax.numpy as jnp
from jax import lax
from jax.sharding import PartitionSpec as P

HEAD = 64
KB = 32
QB = 64
NSEL = 16


def per_device(queries, key_vectors, value_vectors, log_sums, out_grad, layer_input, chosen):
    axis_count = lax.axis_size("kv")
    own_index = lax.axis_index("kv")
    span_rows = queries.shape[0]
    kv_local = key_vectors.shape[1] // HEAD
    group_size = queries.shape[1] // key_vectors.shape[1]
    blocks_here = span_rows // KB
    query_blocks = span_rows // QB
    score_scale = HEAD ** (-0.5)
    half_width = kv_local * HEAD
    pair_width = 2 * half_width
    paired = jnp.concatenate([key_vectors, value_vectors], axis=1)
    owners = jnp.arange(axis_count, dtype=jnp.int32)
    usable = chosen >= 0
    owner_of = jnp.where(usable, chosen // blocks_here, -1)
    within = chosen - chosen // blocks_here * blocks_here
    matched = owner_of[:, :, None] == owners[None, None, :]
    wanted = jnp.max(jnp.where(matched, within[:, :, None], -1), axis=(0, 1))
    incoming = lax.all_to_all(wanted[:, None], "kv", split_axis=0, concat_axis=0, tiled=True)[:, 0]
    blocks = paired.reshape(blocks_here, KB, pair_width)
    outgoing = jnp.where(
        (incoming >= 0)[:, None, None],
        blocks[jnp.maximum(incoming, 0)],
        jnp.zeros((), paired.dtype),
    )
    fetched = lax.all_to_all(outgoing, "kv", split_axis=0, concat_axis=0, tiled=True)
    query_parts = queries.reshape(query_blocks, QB, kv_local, group_size, HEAD)
    grad_parts = out_grad.reshape(query_blocks, QB, kv_local, group_size, HEAD)
    sum_parts = log_sums.reshape(query_blocks, QB, kv_local, group_size)
    slot_owner = jnp.clip(owner_of, 0, axis_count - 1)
    key_own = key_vectors.reshape(span_rows, kv_local, HEAD)
    value_own = value_vectors.reshape(span_rows, kv_local, HEAD)
    key_pos = own_index * span_rows + jnp.arange(span_rows, dtype=jnp.int32)

    def one_block(packed):
        query_part, grad_part, sum_part, slot_part, usable_part, block_index = packed
        selected = fetched[slot_part].reshape(NSEL * KB, 2, kv_local, HEAD)
        key_sel = selected[:, 0]
        value_sel = selected[:, 1]
        keep_key = jnp.repeat(usable_part, KB)
        query_pos = own_index * span_rows + block_index * QB + jnp.arange(QB, dtype=jnp.int32)
        causal = key_pos[None, :] <= query_pos[:, None]
        score_sel = (
            jnp.einsum("qhgd,khd->qhgk", query_part, key_sel, preferred_element_type=jnp.float32)
            * score_scale
        )
        score_own = (
            jnp.einsum("qhgd,khd->qhgk", query_part, key_own, preferred_element_type=jnp.float32)
            * score_scale
        )
        weight_sel = jnp.where(
            keep_key[None, None, None, :], jnp.exp(score_sel - sum_part[..., None]), 0.0
        )
        weight_own = jnp.where(
            causal[:, None, None, :], jnp.exp(score_own - sum_part[..., None]), 0.0
        )
        round_sel = weight_sel.astype(jnp.bfloat16)
        round_own = weight_own.astype(jnp.bfloat16)
        output = jnp.einsum(
            "qhgk,khd->qhgd", round_sel, value_sel, preferred_element_type=jnp.float32
        )
        output = output + jnp.einsum(
            "qhgk,khd->qhgd", round_own, value_own, preferred_element_type=jnp.float32
        )
        row_delta = jnp.sum(grad_part.astype(jnp.float32) * output, axis=-1)
        prod_sel = jnp.einsum(
            "qhgd,khd->qhgk", grad_part, value_sel, preferred_element_type=jnp.float32
        )
        prod_own = jnp.einsum(
            "qhgd,khd->qhgk", grad_part, value_own, preferred_element_type=jnp.float32
        )
        slope_sel = (weight_sel * (prod_sel - row_delta[..., None])).astype(jnp.bfloat16)
        slope_own = (weight_own * (prod_own - row_delta[..., None])).astype(jnp.bfloat16)
        query_total = jnp.einsum(
            "qhgk,khd->qhgd", slope_sel, key_sel, preferred_element_type=jnp.float32
        )
        query_total = query_total + jnp.einsum(
            "qhgk,khd->qhgd", slope_own, key_own, preferred_element_type=jnp.float32
        )
        query_out = (query_total * score_scale).astype(jnp.bfloat16)
        key_sel_grad = (
            jnp.einsum("qhgk,qhgd->khd", slope_sel, query_part, preferred_element_type=jnp.float32)
            * score_scale
        )
        value_sel_grad = jnp.einsum(
            "qhgk,qhgd->khd", round_sel, grad_part, preferred_element_type=jnp.float32
        )
        key_own_grad = (
            jnp.einsum("qhgk,qhgd->khd", slope_own, query_part, preferred_element_type=jnp.float32)
            * score_scale
        )
        value_own_grad = jnp.einsum(
            "qhgk,qhgd->khd", round_own, grad_part, preferred_element_type=jnp.float32
        )
        sel_pair = jnp.concatenate(
            [
                key_sel_grad.reshape(NSEL, KB, half_width),
                value_sel_grad.reshape(NSEL, KB, half_width),
            ],
            axis=2,
        )
        own_pair = jnp.concatenate(
            [
                key_own_grad.reshape(span_rows, half_width),
                value_own_grad.reshape(span_rows, half_width),
            ],
            axis=1,
        )
        return (query_out, sel_pair, own_pair)

    block_ids = jnp.arange(query_blocks, dtype=jnp.int32)
    query_outs, sel_pairs, own_pairs = lax.map(
        one_block, (query_parts, grad_parts, sum_parts, slot_owner, usable, block_ids)
    )
    onehot = ((slot_owner[:, :, None] == owners[None, None, :]) & usable[:, :, None]).astype(
        jnp.float32
    )
    onehot = onehot.reshape(query_blocks * NSEL, axis_count)
    per_owner = jnp.einsum(
        "so,sr->or",
        onehot,
        sel_pairs.reshape(query_blocks * NSEL, KB * pair_width),
        precision=lax.Precision.HIGHEST,
    )
    returned = lax.all_to_all(
        per_owner.reshape(axis_count, KB, pair_width), "kv", split_axis=0, concat_axis=0, tiled=True
    )
    placing = (incoming[None, :] == jnp.arange(blocks_here, dtype=jnp.int32)[:, None]).astype(
        jnp.float32
    )
    landed = jnp.einsum(
        "bs,sr->br",
        placing,
        returned.reshape(axis_count, KB * pair_width),
        precision=lax.Precision.HIGHEST,
    )
    totals = jnp.sum(own_pairs, axis=0) + landed.reshape(span_rows, pair_width)
    key_grad = totals[:, :half_width].astype(jnp.bfloat16)
    value_grad = totals[:, half_width:].astype(jnp.bfloat16)
    full_input = lax.all_gather(layer_input, "tp", axis=1, tiled=True)
    weight_grad = lax.psum_scatter(
        lax.dot_general(
            full_input, key_grad, (((0,), (0,)), ((), ())), preferred_element_type=jnp.float32
        ),
        "kv",
        scatter_dimension=0,
        tiled=True,
    )
    return (query_outs.reshape(span_rows, queries.shape[1]), key_grad, value_grad, weight_grad)


def solution(mesh):
    placed = (
        P("kv", "tp"),
        P("kv", "tp"),
        P("kv", "tp"),
        P("kv", "tp"),
        P("kv", "tp"),
        P("kv", "tp"),
        P("kv", None),
    )
    return jax.shard_map(
        per_device,
        mesh=mesh,
        in_specs=placed,
        out_specs=(P("kv", "tp"), P("kv", "tp"), P("kv", "tp"), P("kv", "tp")),
        check_vma=False,
    )
```

profile of v0, /device:TPU:0, one launch (start us, length us, event | category | flops | bytes accessed | tf_op | source)
XLA Modules:
  0.0 224.7 jit_solution(12152546866315410712)
XLA Ops:
  7.2 1.3 broadcast_clamp_fusion
  9.3 7.3 %all-to-all-start = ((s32[8,1,1]{2,1,0:T(1,128)}), s32[8,1,1]{2,1,0:T(1,128)S(1)}, u32[]{:S(2)}, u32[]{:S(2)}) async-start(s32[8,1,1]{2,1,0:T(1,128)} %copy.110), calls=%async_computation | async-start | bytes 8192 | tf_op jit(solution)/shard_map/all_to_all | solution.py:30
  17.5 5.5 %all-to-all-done = s32[8,1,1]{2,1,0:T(1,128)S(1)} async-done(((s32[8,1,1]{2,1,0:T(1,128)}), s32[8,1,1]{2,1,0:T(1,128)S(1)}, u32[]{:S(2)}, u32[]{:S(2)}) %all-to-all-start) | async-done | bytes 64 | tf_op jit(solution)/shard_map/all_to_all | solution.py:30
  24.9 3.4 %all-to-all-start.1 = ((bf16[8,32,256]{2,1,0:T(8,128)(2,1)}), bf16[8,32,256]{2,1,0:T(8,128)(2,1)S(1)}, u32[]{:S(2)}, u32[]{:S(2)}) async-start(bf16[8,32,256]{2,1,0:T(8,128)(2,1)} %broadcast_select_fusion), calls=%async_computation.1 | async-start | bytes 262144 | tf_op jit(solution)/shard_map/all_to_all | solution.py:37
  29.1 1.6 copy.113
  35.0 1.2 and.19
  36.9 93.2 %while.18 = (s32[]{:T(128)}, bf16[4,64,2,6,64]{1,4,3,2,0:T(8,128)(2,1)}, f32[4,16,32,256]{3,2,1,0:T(8,128)}, f32[4,256,256]{1,2,0:T(8,128)}, s32[4,16]{1,0:T(4,1...) while((s32[]{:T(128)}, ...), condition=%wide.region_3.4_spmd.clone.clone, body=%wide.region_1.3_spmd.clone.clone.sunk | while | flops 458359424 | bytes 25241412 | solution.py:123
  39.2 1.4 fusion.153
  42.5 1.2 fusion.154
  43.8 1.3 fusion.155
  45.1 1.3 fusion.156
  46.3 1.2 fusion.159
  48.6 2.0 reshape.226
  50.6 1.2 convolution_bitcast_fusion.14
  53.7 1.2 fusion.157
  58.5 1.8 fusion.158
  62.5 1.4 fusion.153
  65.8 1.2 fusion.154
  67.0 1.3 fusion.155
  68.3 1.3 fusion.156
  69.6 1.2 fusion.159
  71.9 2.0 reshape.226
  73.9 1.2 convolution_bitcast_fusion.14
  76.9 1.2 fusion.157
  81.7 1.8 fusion.158
  85.8 1.4 fusion.153
  89.0 1.2 fusion.154
  90.3 1.3 fusion.155
  91.6 1.3 fusion.156
  92.9 1.2 fusion.159
  95.1 2.0 reshape.226
  97.2 1.2 convolution_bitcast_fusion.14
  100.2 1.2 fusion.157
  105.0 1.8 fusion.158
  109.1 1.4 fusion.153
  113.6 1.3 fusion.155
  114.9 1.3 fusion.156
  116.2 1.2 fusion.159
  118.4 2.0 reshape.226
  123.5 1.2 fusion.157
  128.3 1.8 fusion.158
  130.1 3.5 %fusion.66 = f32[8,32,256]{2,0,1:T(8,128)S(1)} fusion(s32[64]{0:T(128)} %eq.51, pred[64]{0:T(512)(128)(4,1)} %and.19, f32[8,8,32,256]{3,2,1,0:T(8,128)} %bitcast.274), kind=kOutput, calls=%fused_computation.90 | convolution fusion | flops 50332672 | bytes 2359616 | tf_op jit(solution)/shard_map/so,sr->or/dot_general | solution.py:130
  134.5 5.9 %all-to-all-start.2 = ((f32[8,32,256]{2,1,0:T(8,128)}), f32[8,32,256]{2,1,0:T(8,128)S(1)}, u32[]{:S(2)}, u32[]{:S(2)}) async-start(f32[8,32,256]{2,1,0:T(8,128)} %copy.120), calls=%async_computation.2 | async-start | bytes 524288 | tf_op jit(solution)/shard_map/all_to_all | solution.py:136
  140.7 7.9 %all-to-all-done.2 = f32[8,32,256]{2,1,0:T(8,128)S(1)} async-done(((f32[8,32,256]{2,1,0:T(8,128)}), f32[8,32,256]{2,1,0:T(8,128)S(1)}, u32[]{:S(2)}, u32[]{:S(2)}) %all-to-all-start.2) | async-done | bytes 262176 | tf_op jit(solution)/shard_map/all_to_all | solution.py:136
  149.3 2.9 %convolution_bitcast_fusion.8 = f32[3072,128]{0,1:T(8,128)} fusion(bf16[256,3072]{1,0:T(8,128)(2,1)} %all-gather.2.cloned.1.call-done, bf16[256,256]{0,1:T(8,128)(2,1)S(1)} %add_convert_fusion), kind=kOutput, calls=%fused_computation.89 | convolution fusion | flops 201326592 | bytes 3211264 | tf_op jit(solution)/shard_map/dot_general | solution.py:153
  154.3 1.4 reshape.213
  157.2 58.9 %reduce-scatter.2.cloned.1.call-done = f32[384,128]{0,1:T(8,128)} async-done(((f32[3072,128]{0,1:T(8,128)}), f32[384,128]{0,1:T(8,128)}) %reduce-scatter.2.cloned.1.call-update) | async-done | bytes 196624 | tf_op jit(solution)/shard_map/reduce_scatter | solution.py:152
  216.1 1.7 copy.125
  (206 shorter events, 55.8 us)
Async XLA Ops:
  7.2 23.5 %copy-start.7 = (bf16[256,128]{1,0:T(8,128)(2,1)S(1)}, bf16[256,128]{1,0:T(8,128)(2,1)}, u32[]{:S(2)}) copy-start(bf16[256,128]{1,0:T(8,128)(2,1)} %param.11) | copy-start | bytes 196612
  7.2 24.2 %copy-start.5 = (bf16[256,768]{1,0:T(8,128)(2,1)S(1)}, bf16[256,768]{1,0:T(8,128)(2,1)}, u32[]{:S(2)}) copy-start(bf16[256,768]{1,0:T(8,128)(2,1)} %param.9) | copy-start | bytes 1179652
  9.3 13.7 %all-to-all-start = ((s32[8,1,1]{2,1,0:T(1,128)}), s32[8,1,1]{2,1,0:T(1,128)S(1)}, u32[]{:S(2)}, u32[]{:S(2)}) async-start(s32[8,1,1]{2,1,0:T(1,128)} %copy.110), calls=%async_computation | async-start | bytes 8192 | tf_op jit(solution)/shard_map/all_to_all | solution.py:30
  24.9 12.0 %all-to-all-start.1 = ((bf16[8,32,256]{2,1,0:T(8,128)(2,1)}), bf16[8,32,256]{2,1,0:T(8,128)(2,1)S(1)}, u32[]{:S(2)}, u32[]{:S(2)}) async-start(bf16[8,32,256]{2,1,0:T(8,128)(2,1)} %broadcast_select_fusion), calls=%async_computation.1 | async-start | bytes 262144 | tf_op jit(solution)/shard_map/all_to_all | solution.py:37
  28.3 120.9 %all-gather.2.cloned.1.call-start = ((), (), s32[]{:S(2)}) async-start(), calls=%async_computation.4 | async-start | bytes 1966080 | tf_op jit(solution)/shard_map/all_gather | solution.py:151
  31.4 1.8 copy-start.6
  33.2 1.8 copy-start.10
  36.9 2.3 %copy-start.8 = (f32[4,64,2,6]{1,0,3,2:T(4,128)}, f32[4,64,2,6]{1,0,3,2:T(4,128)S(1)}, u32[]{:S(2)}) copy-start(f32[4,64,2,6]{1,0,3,2:T(4,128)S(1)} %get-tuple-element.488) | copy-start | bytes 36868 | tf_op jit(solution)/shard_map/while
  36.9 4.2 %copy-start.11 = (s32[4]{0:T(128)}, s32[4]{0:T(128)S(1)}, u32[]{:S(2)}) copy-start(s32[4]{0:T(128)S(1)} %get-tuple-element.490) | copy-start | bytes 52 | tf_op jit(solution)/shard_map/while
  38.3 2.3 %copy-start.1 = (bf16[512,1,2,64]{0,3,2,1:T(8,128)(2,1)}, bf16[512,1,2,64]{0,3,2,1:T(8,128)(2,1)S(1)}, u32[]{:S(2)}) copy-start(bf16[512,1,2,64]{0,3,2,1:T(8,128)(2,1)S(1)} %copy.168) | copy-start | bytes 393220 | tf_op jit(solution)/shard_map/while
  51.9 1.0 copy-start
  53.6 4.3 %copy-start.2 = (bf16[512,1,2,64]{0,3,2,1:T(8,128)(2,1)S(1)}, bf16[512,1,2,64]{0,3,2,1:T(8,128)(2,1)}, u32[]{:S(2)}) copy-start(bf16[512,1,2,64]{0,3,2,1:T(8,128)(2,1)} %copy-done.1) | copy-start | bytes 393220 | tf_op jit(solution)/shard_map/while
  57.2 3.1 %copy-start.9 = (f32[4,64,2,6]{1,0,3,2:T(4,128)S(1)}, f32[4,64,2,6]{1,0,3,2:T(4,128)}, u32[]{:S(2)}) copy-start(f32[4,64,2,6]{1,0,3,2:T(4,128)} %copy-done.8) | copy-start | bytes 36868 | tf_op jit(solution)/shard_map/while
  57.2 3.1 %copy-start.12 = (s32[4]{0:T(128)S(1)}, s32[4]{0:T(128)}, u32[]{:S(2)}) copy-start(s32[4]{0:T(128)} %copy-done.11) | copy-start | bytes 52 | tf_op jit(solution)/shard_map/while
  60.3 2.3 %copy-start.8 = (f32[4,64,2,6]{1,0,3,2:T(4,128)}, f32[4,64,2,6]{1,0,3,2:T(4,128)S(1)}, u32[]{:S(2)}) copy-start(f32[4,64,2,6]{1,0,3,2:T(4,128)S(1)} %get-tuple-element.488) | copy-start | bytes 36868 | tf_op jit(solution)/shard_map/while
  60.3 4.1 %copy-start.11 = (s32[4]{0:T(128)}, s32[4]{0:T(128)S(1)}, u32[]{:S(2)}) copy-start(s32[4]{0:T(128)S(1)} %get-tuple-element.490) | copy-start | bytes 52 | tf_op jit(solution)/shard_map/while
  61.7 2.2 copy-start.1
  75.1 1.0 copy-start
  76.9 4.3 %copy-start.2 = (bf16[512,1,2,64]{0,3,2,1:T(8,128)(2,1)S(1)}, bf16[512,1,2,64]{0,3,2,1:T(8,128)(2,1)}, u32[]{:S(2)}) copy-start(bf16[512,1,2,64]{0,3,2,1:T(8,128)(2,1)} %copy-done.1) | copy-start | bytes 393220 | tf_op jit(solution)/shard_map/while
  80.5 3.1 %copy-start.9 = (f32[4,64,2,6]{1,0,3,2:T(4,128)S(1)}, f32[4,64,2,6]{1,0,3,2:T(4,128)}, u32[]{:S(2)}) copy-start(f32[4,64,2,6]{1,0,3,2:T(4,128)} %copy-done.8) | copy-start | bytes 36868 | tf_op jit(solution)/shard_map/while
  80.5 3.1 %copy-start.12 = (s32[4]{0:T(128)S(1)}, s32[4]{0:T(128)}, u32[]{:S(2)}) copy-start(s32[4]{0:T(128)} %copy-done.11) | copy-start | bytes 52 | tf_op jit(solution)/shard_map/while
  83.5 2.3 %copy-start.8 = (f32[4,64,2,6]{1,0,3,2:T(4,128)}, f32[4,64,2,6]{1,0,3,2:T(4,128)S(1)}, u32[]{:S(2)}) copy-start(f32[4,64,2,6]{1,0,3,2:T(4,128)S(1)} %get-tuple-element.488) | copy-start | bytes 36868 | tf_op jit(solution)/shard_map/while
  83.5 4.1 %copy-start.11 = (s32[4]{0:T(128)}, s32[4]{0:T(128)S(1)}, u32[]{:S(2)}) copy-start(s32[4]{0:T(128)S(1)} %get-tuple-element.490) | copy-start | bytes 52 | tf_op jit(solution)/shard_map/while
  84.9 2.2 copy-start.1
  98.4 1.0 copy-start
  100.2 4.3 %copy-start.2 = (bf16[512,1,2,64]{0,3,2,1:T(8,128)(2,1)S(1)}, bf16[512,1,2,64]{0,3,2,1:T(8,128)(2,1)}, u32[]{:S(2)}) copy-start(bf16[512,1,2,64]{0,3,2,1:T(8,128)(2,1)} %copy-done.1) | copy-start | bytes 393220 | tf_op jit(solution)/shard_map/while
  103.8 3.1 %copy-start.9 = (f32[4,64,2,6]{1,0,3,2:T(4,128)S(1)}, f32[4,64,2,6]{1,0,3,2:T(4,128)}, u32[]{:S(2)}) copy-start(f32[4,64,2,6]{1,0,3,2:T(4,128)} %copy-done.8) | copy-start | bytes 36868 | tf_op jit(solution)/shard_map/while
  103.8 3.1 %copy-start.12 = (s32[4]{0:T(128)S(1)}, s32[4]{0:T(128)}, u32[]{:S(2)}) copy-start(s32[4]{0:T(128)} %copy-done.11) | copy-start | bytes 52 | tf_op jit(solution)/shard_map/while
  106.9 2.3 %copy-start.8 = (f32[4,64,2,6]{1,0,3,2:T(4,128)}, f32[4,64,2,6]{1,0,3,2:T(4,128)S(1)}, u32[]{:S(2)}) copy-start(f32[4,64,2,6]{1,0,3,2:T(4,128)S(1)} %get-tuple-element.488) | copy-start | bytes 36868 | tf_op jit(solution)/shard_map/while
  106.9 4.1 %copy-start.11 = (s32[4]{0:T(128)}, s32[4]{0:T(128)S(1)}, u32[]{:S(2)}) copy-start(s32[4]{0:T(128)S(1)} %get-tuple-element.490) | copy-start | bytes 52 | tf_op jit(solution)/shard_map/while
  108.2 2.2 copy-start.1
  121.7 1.0 copy-start
  123.5 4.3 %copy-start.2 = (bf16[512,1,2,64]{0,3,2,1:T(8,128)(2,1)S(1)}, bf16[512,1,2,64]{0,3,2,1:T(8,128)(2,1)}, u32[]{:S(2)}) copy-start(bf16[512,1,2,64]{0,3,2,1:T(8,128)(2,1)} %copy-done.1) | copy-start | bytes 393220 | tf_op jit(solution)/shard_map/while
  127.0 3.1 %copy-start.9 = (f32[4,64,2,6]{1,0,3,2:T(4,128)S(1)}, f32[4,64,2,6]{1,0,3,2:T(4,128)}, u32[]{:S(2)}) copy-start(f32[4,64,2,6]{1,0,3,2:T(4,128)} %copy-done.8) | copy-start | bytes 36868 | tf_op jit(solution)/shard_map/while
  127.0 3.1 %copy-start.12 = (s32[4]{0:T(128)S(1)}, s32[4]{0:T(128)}, u32[]{:S(2)}) copy-start(s32[4]{0:T(128)} %copy-done.11) | copy-start | bytes 52 | tf_op jit(solution)/shard_map/while
  130.1 10.5 %copy-start.3 = (f32[4,256,256]{1,2,0:T(8,128)S(1)}, f32[4,256,256]{1,2,0:T(8,128)}, u32[]{:S(2)}) copy-start(f32[4,256,256]{1,2,0:T(8,128)} %get-tuple-element.178) | copy-start | bytes 3145732
  134.5 14.1 %all-to-all-start.2 = ((f32[8,32,256]{2,1,0:T(8,128)}), f32[8,32,256]{2,1,0:T(8,128)S(1)}, u32[]{:S(2)}, u32[]{:S(2)}) async-start(f32[8,32,256]{2,1,0:T(8,128)} %copy.120), calls=%async_computation.2 | async-start | bytes 524288 | tf_op jit(solution)/shard_map/all_to_all | solution.py:136
  140.4 75.8 %reduce-scatter.2.cloned.1.call-start = ((), (), s32[]{:S(2)}) async-start(), calls=%async_computation.5 | async-start | bytes 1769472 | tf_op jit(solution)/shard_map/reduce_scatter | solution.py:152
  152.2 1.1 copy-start.4
Sparse Core Ops, SparseCore 0:
  30.7 20.9 all-gather.1
  152.3 63.7 reduce-scatter.1
where the time goes:
time: 227 us; the launch traced here: 225 us
  waiting for transfers between devices  73.1 us (32%)
  matrix products  62.1 us (27%)
  local copies, waits for them, and re-layouts  44.4 us (20%)
  starting transfers between devices  16.9 us (7%)
  between operations  14.2 us (6%)
  other arithmetic  10.4 us (5%)
  loops' own time  3.57 us (2%)
    reduce_scatter x1, waiting for transfers between devices, per_device(): lax.psum_scatter(lax.dot_general(full_input, key_grad, (((0,), (0,)), (()...  58.9 us
    unnamed x22, local copies, waits for them, and re-layouts  11.4 us
    reshape x4, local copies, waits for them, and re-layouts, one_block(): key_sel_grad.reshape(NSEL, KB, half_width)  8.17 us
    all_to_all x1, waiting for transfers between devices, per_device(): lax.all_to_all(per_owner.reshape(axis_count, KB, pair_width), 'kv', split...  7.9 us
    dot_general x4, matrix products, one_block(): jnp.einsum('qhgk,khd->qhgd', slope_own, key_own, preferred_element_type=j...  7.34 us
    all_to_all x1, starting transfers between devices, per_device(): lax.all_to_all(wanted[:, None], 'kv', split_axis=0, concat_axis=0, tiled=...  7.31 us
    dynamic_update_slice x8, other arithmetic, per_device(): lax.map(one_block, (query_parts, grad_parts, sum_parts, slot_owner, usabl...  6.22 us
    all_to_all x1, starting transfers between devices, per_device(): lax.all_to_all(per_owner.reshape(axis_count, KB, pair_width), 'kv', split...  5.91 us
  transfers between devices with their start and end apart: 5, of which 3 were waited for; matrix products, arithmetic and copies ran while one was open for 47% of the time, Pallas kernels for 0%

commit v1 on v0

--- a/solution.py
+++ b/solution.py
@@ -7,6 +7,29 @@
 KB = 32
 QB = 64
 NSEL = 16
+
+
+def in_blocks(shard, dim, size):
+    dims = shard.shape
+    blocks = shard.reshape(*dims[:dim], size, dims[dim] // size, *dims[dim + 1 :])
+    return jnp.moveaxis(blocks, dim, 0)
+
+
+def joined_along(parts, dim):
+    parts = jnp.moveaxis(parts, 0, dim)
+    lengths = parts.shape
+    return parts.reshape(*lengths[:dim], lengths[dim] * lengths[dim + 1], *lengths[dim + 2 :])
+
+
+def exchange_directly(x, axis, split_dim, concat_dim):
+    length, index = (lax.axis_size(axis), lax.axis_index(axis))
+    pieces = in_blocks(x, split_dim, length)
+    outs = [pieces[index]]
+    for step in range(1, length):
+        sent = pieces[(index + step) % length]
+        outs.append(lax.ppermute(sent, axis, [(i, (i + step) % length) for i in range(length)]))
+    pieces = jnp.stack(outs)[(index - jnp.arange(length)) % length]
+    return joined_along(pieces, concat_dim)
 
 
 def per_device(queries, key_vectors, value_vectors, log_sums, out_grad, layer_input, chosen):
@@ -27,7 +50,7 @@
     within = chosen - chosen // blocks_here * blocks_here
     matched = owner_of[:, :, None] == owners[None, None, :]
     wanted = jnp.max(jnp.where(matched, within[:, :, None], -1), axis=(0, 1))
-    incoming = lax.all_to_all(wanted[:, None], "kv", split_axis=0, concat_axis=0, tiled=True)[:, 0]
+    incoming = exchange_directly(wanted[:, None], "kv", 0, 0)[:, 0]
     blocks = paired.reshape(blocks_here, KB, pair_width)
     outgoing = jnp.where(
         (incoming >= 0)[:, None, None],

time: 227 us -> 236 us (1.040)
  starting transfers between devices: 16.9 us -> 25.1 us
  local copies, waits for them, and re-layouts: 44.4 us -> 49.7 us
  waiting for transfers between devices: 73.1 us -> 69.6 us
    ppermute x0 -> x7, starting transfers between devices: none -> 13.8 us  [exchange_directly(): lax.ppermute(sent, axis, [(i, (i + step) % length) for i in range(length)])]
    all_to_all x1 -> x0, starting transfers between devices: 7.31 us -> none  [per_device(): lax.all_to_all(wanted[:, None], 'kv', split_axis=0, concat_axis=0, tiled=...]
    all_to_all x1 -> x0, waiting for transfers between devices: 5.53 us -> none  [per_device(): lax.all_to_all(wanted[:, None], 'kv', split_axis=0, concat_axis=0, tiled=...]
    another operation x0 -> x1, local copies, waits for them, and re-layouts: none -> 5.27 us  [exchange_directly(): pieces = jnp.stack(outs)[(index - jnp.arange(length)) % length]]
    unnamed x22 -> x24, local copies, waits for them, and re-layouts: 11.4 us -> 10.5 us
  transfers between devices with their start and end apart: 5 -> 11, of which waited for: 3 -> 4; matrix products, arithmetic and copies ran while one was open for 47% -> 45% of each run, Pallas kernels for 0% -> 0%
where the time goes in v1:
time: 236 us; the launch traced here: 234 us
  waiting for transfers between devices  69.6 us (29%)
  matrix products  62.2 us (26%)
  local copies, waits for them, and re-layouts  49.7 us (21%)
  starting transfers between devices  25.1 us (11%)
  between operations  14.3 us (6%)
  other arithmetic  9.91 us (4%)
  loops' own time  3.57 us (2%)
    reduce_scatter x1, waiting for transfers between devices, per_device(): lax.psum_scatter(lax.dot_general(full_input, key_grad, (((0,), (0,)), (()...  59.2 us
    ppermute x7, starting transfers between devices, exchange_directly(): lax.ppermute(sent, axis, [(i, (i + step) % length) for i in range(length)])  13.8 us
    unnamed x24, local copies, waits for them, and re-layouts  10.5 us
    reshape x4, local copies, waits for them, and re-layouts, one_block(): key_sel_grad.reshape(NSEL, KB, half_width)  8.19 us
    all_to_all x1, waiting for transfers between devices, per_device(): lax.all_to_all(per_owner.reshape(axis_count, KB, pair_width), 'kv', split...  7.9 us
    dot_general x4, matrix products, one_block(): jnp.einsum('qhgk,khd->qhgd', slope_own, key_own, preferred_element_type=j...  7.41 us
    dynamic_update_slice x8, other arithmetic, per_device(): lax.map(one_block, (query_parts, grad_parts, sum_parts, slot_owner, usabl...  6.28 us
    all_to_all x1, starting transfers between devices, per_device(): lax.all_to_all(per_owner.reshape(axis_count, KB, pair_width), 'kv', split...  5.95 us
  transfers between devices with their start and end apart: 11, of which 4 were waited for; matrix products, arithmetic and copies ran while one was open for 45% of the time, Pallas kernels for 0%

profile of v1, /device:TPU:0, one launch (start us, length us, event | category | flops | bytes accessed | tf_op | source)
XLA Modules:
  0.0 234.4 jit_solution(4898858602396066675)
XLA Ops:
  7.3 1.3 broadcast_clamp_fusion
  9.4 5.0 %collective-permute-start.4 = (s32[1,1]{1,0:T(1,128)}, s32[1,1]{1,0:T(1,128)}, u32[]{:S(2)}, u32[]{:S(2)}) collective-permute-start(s32[1,1]{1,0:T(1,128)} %bitcast.9), channel_id=1, source_target_pairs={{0,20},{4,24},{8,28},{12,0},{16,4},{20,8},{24,12},{28,16},{1,21},{... | collective-permute-start | bytes 20 | tf_op jit(solution)/shard_map/ppermute | solution.py:30
  14.4 1.3 collective-permute-start.5
  16.3 1.5 collective-permute-start
  19.4 1.9 collective-permute-start.2
  21.3 2.8 %collective-permute-start.3 = (s32[1,1]{1,0:T(1,128)}, s32[1,1]{1,0:T(1,128)}, u32[]{:S(2)}, u32[]{:S(2)}) collective-permute-start(s32[1,1]{1,0:T(1,128)} %bitcast.7), channel_id=1, source_target_pairs={{0,16},{4,20},{8,24},{12,28},{16,0},{20,4},{24,8},{28,12},{1,17},{... | collective-permute-start | bytes 20 | tf_op jit(solution)/shard_map/ppermute | solution.py:30
  25.9 5.3 %stack.31 = s32[8,1,1]{0,2,1:T(1,128)S(1)} concatenate(s32[1,1,1]{0,2,1:T(1,128)} %bitcast, s32[1,1,1]{0,2,1:T(1,128)} %bitcast.2, s32[1,1,1]{0,2,1:T(1,128)} %bitcast.4, s32[1,1,1]{0,2,1:T(1,128)} %bitcast.6, s32[1,1,1]{0,2,1:T(1,128)} %bitcast.8, s32[1,1,1]{0,2,1:T(1,128)} %bitcast.10, s32[1,1,1]{0,2,1:T(1,128)} %bitcast.12, s32[1,1,1]{0,2,1:T(1,128)} %bitcast.14), dimensions={0} | concatenate | bytes 64 | tf_op jit(solution)/shard_map/stack | solution.py:31
  33.1 5.1 %all-to-all-start = ((bf16[8,32,256]{2,1,0:T(8,128)(2,1)}), bf16[8,32,256]{2,1,0:T(8,128)(2,1)S(1)}, u32[]{:S(2)}, u32[]{:S(2)}) async-start(bf16[8,32,256]{2,1,0:T(8,128)(2,1)} %broadcast_select_fusion), calls=%async_computation | async-start | bytes 262144 | tf_op jit(solution)/shard_map/all_to_all | solution.py:60
  44.1 1.3 and.74
  46.1 93.4 %while.18 = (s32[]{:T(128)}, bf16[4,64,2,6,64]{1,4,3,2,0:T(8,128)(2,1)}, f32[4,16,32,256]{3,2,1,0:T(8,128)}, f32[4,256,256]{1,2,0:T(8,128)}, s32[4,16]{1,0:T(4,1...) while((s32[]{:T(128)}, ...), condition=%wide.region_3.4_spmd.clone.clone, body=%wide.region_1.3_spmd.clone.clone.sunk | while | flops 458359424 | bytes 25241412 | solution.py:146
  48.4 1.4 fusion.155
  51.7 1.2 fusion.156
  52.9 1.3 fusion.157
  54.2 1.3 fusion.158
  55.5 1.2 fusion.161
  57.7 2.1 reshape.303
  59.8 1.2 convolution_bitcast_fusion.14
  62.8 1.2 fusion.159
  67.6 1.8 fusion.160
  71.8 1.4 fusion.155
  76.2 1.3 fusion.157
  77.5 1.3 fusion.158
  78.8 1.2 fusion.161
  81.1 2.0 reshape.303
  86.1 1.2 fusion.159
  90.9 1.9 fusion.160
  95.1 1.4 fusion.155
  99.6 1.3 fusion.157
  100.9 1.3 fusion.158
  102.2 1.2 fusion.161
  104.4 2.0 reshape.303
  106.4 1.2 convolution_bitcast_fusion.14
  114.3 1.9 fusion.160
  118.4 1.4 fusion.155
  121.7 1.2 fusion.156
  122.9 1.3 fusion.157
  124.2 1.3 fusion.158
  125.5 1.2 fusion.161
  127.7 2.0 reshape.303
  132.8 1.2 fusion.159
  137.6 1.8 fusion.160
  139.5 3.5 %fusion.66 = f32[8,32,256]{2,0,1:T(8,128)S(1)} fusion(s32[64]{0:T(128)} %eq.58, pred[64]{0:T(512)(128)(4,1)} %and.74, f32[8,8,32,256]{3,2,1,0:T(8,128)} %bitcast.292), kind=kOutput, calls=%fused_computation.91 | convolution fusion | flops 50332672 | bytes 2359616 | tf_op jit(solution)/shard_map/so,sr->or/dot_general | solution.py:153
  143.8 6.0 %all-to-all-start.1 = ((f32[8,32,256]{2,1,0:T(8,128)}), f32[8,32,256]{2,1,0:T(8,128)S(1)}, u32[]{:S(2)}, u32[]{:S(2)}) async-start(f32[8,32,256]{2,1,0:T(8,128)} %copy.91), calls=%async_computation.1 | async-start | bytes 524288 | tf_op jit(solution)/shard_map/all_to_all | solution.py:159
  150.1 7.9 %all-to-all-done.1 = f32[8,32,256]{2,1,0:T(8,128)S(1)} async-done(((f32[8,32,256]{2,1,0:T(8,128)}), f32[8,32,256]{2,1,0:T(8,128)S(1)}, u32[]{:S(2)}, u32[]{:S(2)}) %all-to-all-start.1) | async-done | bytes 262176 | tf_op jit(solution)/shard_map/all_to_all | solution.py:159
  158.7 2.9 %convolution_bitcast_fusion.8 = f32[3072,128]{0,1:T(8,128)} fusion(bf16[256,3072]{1,0:T(8,128)(2,1)} %all-gather.2.cloned.1.call-done, bf16[256,256]{0,1:T(8,128)(2,1)S(1)} %add_convert_fusion), kind=kOutput, calls=%fused_computation.90 | convolution fusion | flops 201326592 | bytes 3211264 | tf_op jit(solution)/shard_map/dot_general | solution.py:176
  163.7 1.4 reshape.293
  166.6 59.2 %reduce-scatter.2.cloned.1.call-done = f32[384,128]{0,1:T(8,128)} async-done(((f32[3072,128]{0,1:T(8,128)}), f32[384,128]{0,1:T(8,128)}) %reduce-scatter.2.cloned.1.call-update) | async-done | bytes 196624 | tf_op jit(solution)/shard_map/reduce_scatter | solution.py:175
  225.8 1.7 copy.96
  (224 shorter events, 63.3 us)
Async XLA Ops:
  7.2 31.8 %copy-start.7 = (bf16[256,128]{1,0:T(8,128)(2,1)S(1)}, bf16[256,128]{1,0:T(8,128)(2,1)}, u32[]{:S(2)}) copy-start(bf16[256,128]{1,0:T(8,128)(2,1)} %param.10) | copy-start | bytes 196612
  7.2 32.6 %copy-start.8 = (bf16[256,128]{1,0:T(8,128)(2,1)S(1)}, bf16[256,128]{1,0:T(8,128)(2,1)}, u32[]{:S(2)}) copy-start(bf16[256,128]{1,0:T(8,128)(2,1)} %param.11) | copy-start | bytes 196612
  7.2 33.3 %copy-start.5 = (bf16[256,768]{1,0:T(8,128)(2,1)S(1)}, bf16[256,768]{1,0:T(8,128)(2,1)}, u32[]{:S(2)}) copy-start(bf16[256,768]{1,0:T(8,128)(2,1)} %param.9) | copy-start | bytes 1179652
  9.4 10.0 %collective-permute-start.4 = (s32[1,1]{1,0:T(1,128)}, s32[1,1]{1,0:T(1,128)}, u32[]{:S(2)}, u32[]{:S(2)}) collective-permute-start(s32[1,1]{1,0:T(1,128)} %bitcast.9), channel_id=1, source_target_pairs={{0,20},{4,24},{8,28},{12,0},{16,4},{20,8},{24,12},{28,16},{1,21},{... | collective-permute-start | bytes 20 | tf_op jit(solution)/shard_map/ppermute | solution.py:30
  14.4 6.9 %collective-permute-start.5 = (s32[1,1]{1,0:T(1,128)}, s32[1,1]{1,0:T(1,128)}, u32[]{:S(2)}, u32[]{:S(2)}) collective-permute-start(s32[1,1]{1,0:T(1,128)} %bitcast.11), channel_id=1, source_target_pairs={{0,24},{4,28},{8,0},{12,4},{16,8},{20,12},{24,16},{28,20},{1,25},{... | collective-permute-start | bytes 20 | tf_op jit(solution)/shard_map/ppermute | solution.py:30
  15.8 8.4 %collective-permute-start.6 = (s32[1,1]{1,0:T(1,128)}, s32[1,1]{1,0:T(1,128)}, u32[]{:S(2)}, u32[]{:S(2)}) collective-permute-start(s32[1,1]{1,0:T(1,128)} %bitcast.13), channel_id=1, source_target_pairs={{0,28},{4,0},{8,4},{12,8},{16,12},{20,16},{24,20},{28,24},{1,29},{... | collective-permute-start | bytes 20 | tf_op jit(solution)/shard_map/ppermute | solution.py:30
  16.3 7.9 %collective-permute-start = (s32[1,1]{1,0:T(1,128)}, s32[1,1]{1,0:T(1,128)}, u32[]{:S(2)}, u32[]{:S(2)}) collective-permute-start(s32[1,1]{1,0:T(1,128)} %bitcast.1), channel_id=1, source_target_pairs={{0,4},{4,8},{8,12},{12,16},{16,20},{20,24},{24,28},{28,0},{1,5},{5... | collective-permute-start | bytes 20 | tf_op jit(solution)/shard_map/ppermute | solution.py:30
  17.8 6.3 %collective-permute-start.1 = (s32[1,1]{1,0:T(1,128)}, s32[1,1]{1,0:T(1,128)}, u32[]{:S(2)}, u32[]{:S(2)}) collective-permute-start(s32[1,1]{1,0:T(1,128)} %bitcast.3), channel_id=1, source_target_pairs={{0,8},{4,12},{8,16},{12,20},{16,24},{20,28},{24,0},{28,4},{1,9},{5... | collective-permute-start | bytes 20 | tf_op jit(solution)/shard_map/ppermute | solution.py:30
  19.4 5.4 %collective-permute-start.2 = (s32[1,1]{1,0:T(1,128)}, s32[1,1]{1,0:T(1,128)}, u32[]{:S(2)}, u32[]{:S(2)}) collective-permute-start(s32[1,1]{1,0:T(1,128)} %bitcast.5), channel_id=1, source_target_pairs={{0,12},{4,16},{8,20},{12,24},{16,28},{20,0},{24,4},{28,8},{1,13},{... | collective-permute-start | bytes 20 | tf_op jit(solution)/shard_map/ppermute | solution.py:30
  21.3 4.6 %collective-permute-start.3 = (s32[1,1]{1,0:T(1,128)}, s32[1,1]{1,0:T(1,128)}, u32[]{:S(2)}, u32[]{:S(2)}) collective-permute-start(s32[1,1]{1,0:T(1,128)} %bitcast.7), channel_id=1, source_target_pairs={{0,16},{4,20},{8,24},{12,28},{16,0},{20,4},{24,8},{28,12},{1,17},{... | collective-permute-start | bytes 20 | tf_op jit(solution)/shard_map/ppermute | solution.py:30
  33.1 13.0 %all-to-all-start = ((bf16[8,32,256]{2,1,0:T(8,128)(2,1)}), bf16[8,32,256]{2,1,0:T(8,128)(2,1)S(1)}, u32[]{:S(2)}, u32[]{:S(2)}) async-start(bf16[8,32,256]{2,1,0:T(8,128)(2,1)} %broadcast_select_fusion), calls=%async_computation | async-start | bytes 262144 | tf_op jit(solution)/shard_map/all_to_all | solution.py:60
  38.2 120.4 %all-gather.2.cloned.1.call-start = ((), (), s32[]{:S(2)}) async-start(), calls=%async_computation.3 | async-start | bytes 1966080 | tf_op jit(solution)/shard_map/all_gather | solution.py:174
  40.5 1.8 copy-start.6
  42.3 1.8 copy-start.11
  46.1 2.3 copy-start.9
  46.1 4.2 %copy-start.12 = (s32[4]{0:T(128)}, s32[4]{0:T(128)S(1)}, u32[]{:S(2)}) copy-start(s32[4]{0:T(128)S(1)} %get-tuple-element.478) | copy-start | bytes 52 | tf_op jit(solution)/shard_map/while
  47.5 2.3 copy-start.1
  61.0 1.0 copy-start
  62.8 4.3 %copy-start.2 = (bf16[512,1,2,64]{0,3,2,1:T(8,128)(2,1)S(1)}, bf16[512,1,2,64]{0,3,2,1:T(8,128)(2,1)}, u32[]{:S(2)}) copy-start(bf16[512,1,2,64]{0,3,2,1:T(8,128)(2,1)} %copy-done.1) | copy-start | bytes 393220 | tf_op jit(solution)/shard_map/while
  66.4 3.1 %copy-start.10 = (f32[4,64,2,6]{1,0,3,2:T(4,128)S(1)}, f32[4,64,2,6]{1,0,3,2:T(4,128)}, u32[]{:S(2)}) copy-start(f32[4,64,2,6]{1,0,3,2:T(4,128)} %copy-done.9) | copy-start | bytes 36868 | tf_op jit(solution)/shard_map/while
  66.4 3.1 %copy-start.13 = (s32[4]{0:T(128)S(1)}, s32[4]{0:T(128)}, u32[]{:S(2)}) copy-start(s32[4]{0:T(128)} %copy-done.12) | copy-start | bytes 52 | tf_op jit(solution)/shard_map/while
  69.5 2.3 copy-start.9
  69.5 4.2 %copy-start.12 = (s32[4]{0:T(128)}, s32[4]{0:T(128)S(1)}, u32[]{:S(2)}) copy-start(s32[4]{0:T(128)S(1)} %get-tuple-element.478) | copy-start | bytes 52 | tf_op jit(solution)/shard_map/while
  70.9 2.3 copy-start.1
  84.3 1.0 copy-start
  86.1 4.3 %copy-start.2 = (bf16[512,1,2,64]{0,3,2,1:T(8,128)(2,1)S(1)}, bf16[512,1,2,64]{0,3,2,1:T(8,128)(2,1)}, u32[]{:S(2)}) copy-start(bf16[512,1,2,64]{0,3,2,1:T(8,128)(2,1)} %copy-done.1) | copy-start | bytes 393220 | tf_op jit(solution)/shard_map/while
  89.7 3.1 %copy-start.10 = (f32[4,64,2,6]{1,0,3,2:T(4,128)S(1)}, f32[4,64,2,6]{1,0,3,2:T(4,128)}, u32[]{:S(2)}) copy-start(f32[4,64,2,6]{1,0,3,2:T(4,128)} %copy-done.9) | copy-start | bytes 36868 | tf_op jit(solution)/shard_map/while
  89.7 3.1 %copy-start.13 = (s32[4]{0:T(128)S(1)}, s32[4]{0:T(128)}, u32[]{:S(2)}) copy-start(s32[4]{0:T(128)} %copy-done.12) | copy-start | bytes 52 | tf_op jit(solution)/shard_map/while
  92.8 2.3 copy-start.9
  92.8 4.2 %copy-start.12 = (s32[4]{0:T(128)}, s32[4]{0:T(128)S(1)}, u32[]{:S(2)}) copy-start(s32[4]{0:T(128)S(1)} %get-tuple-element.478) | copy-start | bytes 52 | tf_op jit(solution)/shard_map/while
  94.2 2.3 copy-start.1
  107.7 1.0 copy-start
  109.4 4.3 %copy-start.2 = (bf16[512,1,2,64]{0,3,2,1:T(8,128)(2,1)S(1)}, bf16[512,1,2,64]{0,3,2,1:T(8,128)(2,1)}, u32[]{:S(2)}) copy-start(bf16[512,1,2,64]{0,3,2,1:T(8,128)(2,1)} %copy-done.1) | copy-start | bytes 393220 | tf_op jit(solution)/shard_map/while
  113.0 3.1 %copy-start.10 = (f32[4,64,2,6]{1,0,3,2:T(4,128)S(1)}, f32[4,64,2,6]{1,0,3,2:T(4,128)}, u32[]{:S(2)}) copy-start(f32[4,64,2,6]{1,0,3,2:T(4,128)} %copy-done.9) | copy-start | bytes 36868 | tf_op jit(solution)/shard_map/while
  113.0 3.1 %copy-start.13 = (s32[4]{0:T(128)S(1)}, s32[4]{0:T(128)}, u32[]{:S(2)}) copy-start(s32[4]{0:T(128)} %copy-done.12) | copy-start | bytes 52 | tf_op jit(solution)/shard_map/while
  116.1 2.3 copy-start.9
  116.1 4.2 %copy-start.12 = (s32[4]{0:T(128)}, s32[4]{0:T(128)S(1)}, u32[]{:S(2)}) copy-start(s32[4]{0:T(128)S(1)} %get-tuple-element.478) | copy-start | bytes 52 | tf_op jit(solution)/shard_map/while
  117.5 2.3 copy-start.1
  131.0 1.0 copy-start
  132.8 4.3 %copy-start.2 = (bf16[512,1,2,64]{0,3,2,1:T(8,128)(2,1)S(1)}, bf16[512,1,2,64]{0,3,2,1:T(8,128)(2,1)}, u32[]{:S(2)}) copy-start(bf16[512,1,2,64]{0,3,2,1:T(8,128)(2,1)} %copy-done.1) | copy-start | bytes 393220 | tf_op jit(solution)/shard_map/while
  136.4 3.1 %copy-start.10 = (f32[4,64,2,6]{1,0,3,2:T(4,128)S(1)}, f32[4,64,2,6]{1,0,3,2:T(4,128)}, u32[]{:S(2)}) copy-start(f32[4,64,2,6]{1,0,3,2:T(4,128)} %copy-done.9) | copy-start | bytes 36868 | tf_op jit(solution)/shard_map/while
  136.4 3.1 %copy-start.13 = (s32[4]{0:T(128)S(1)}, s32[4]{0:T(128)}, u32[]{:S(2)}) copy-start(s32[4]{0:T(128)} %copy-done.12) | copy-start | bytes 52 | tf_op jit(solution)/shard_map/while
  139.5 10.5 %copy-start.3 = (f32[4,256,256]{1,2,0:T(8,128)S(1)}, f32[4,256,256]{1,2,0:T(8,128)}, u32[]{:S(2)}) copy-start(f32[4,256,256]{1,2,0:T(8,128)} %get-tuple-element.178) | copy-start | bytes 3145732
  143.8 14.2 %all-to-all-start.1 = ((f32[8,32,256]{2,1,0:T(8,128)}), f32[8,32,256]{2,1,0:T(8,128)S(1)}, u32[]{:S(2)}, u32[]{:S(2)}) async-start(f32[8,32,256]{2,1,0:T(8,128)} %copy.91), calls=%async_computation.1 | async-start | bytes 524288 | tf_op jit(solution)/shard_map/all_to_all | solution.py:159
  149.8 76.0 %reduce-scatter.2.cloned.1.call-start = ((), (), s32[]{:S(2)}) async-start(), calls=%async_computation.4 | async-start | bytes 1769472 | tf_op jit(solution)/shard_map/reduce_scatter | solution.py:175
  161.6 1.1 copy-start.4
Sparse Core Ops, SparseCore 0:
  40.6 21.0 all-gather.1
  161.8 64.0 reduce-scatter.1
